TPU v7x, 32 devices: a whole 2x2x4 slice. The times are simulated.
32 devices in a mesh: sp: 8 (over z, y), tp: 4 (over x, core).
Axes of the slice: x: 2, y: 2, z: 4, core: 2. Of those that a mesh axis runs over, the one named last changes fastest.
Arguments:
- tokens: bfloat16 [1024, 1024], P('sp', 'tp'), may hold values from -6 to 6
- norm_gain: float32 [1024], replicated, may hold values from 0.1 to 1.9
- attn_query: bfloat16 [1024, 512], P('sp', 'tp'), may hold values from -0.1875 to 0.1875
- attn_key: bfloat16 [1024, 256], P('sp', 'tp'), may hold values from -0.1875 to 0.1875
- attn_value: bfloat16 [1024, 256], P('sp', 'tp'), may hold values from -0.1875 to 0.1875
- sink_logit: float32 [8], P('tp'), may hold values from 2 to 7
- delta_query: bfloat16 [1024, 512], P('sp', 'tp'), may hold values from -0.1875 to 0.1875
- delta_key: bfloat16 [1024, 512], P('sp', 'tp'), may hold values from -0.1875 to 0.1875
- delta_value: bfloat16 [1024, 512], P('sp', 'tp'), may hold values from -0.1875 to 0.1875
- delta_gate: bfloat16 [1024, 512], P('sp', 'tp'), may hold values from -0.1875 to 0.1875
- beta_weight: bfloat16 [1024, 8, 2], P('sp', 'tp'), may hold values from -0.1875 to 0.1875
- decay_weight: bfloat16 [1024, 8, 2], P('sp', 'tp'), may hold values from -0.1875 to 0.1875
- beta_shift: float32 [2, 8], P(None, 'tp'), may hold values from -5 to -2
- decay_log: float32 [2, 8], P(None, 'tp'), may hold values from -2.5 to 1
- out_gain: float32 [64], replicated, may hold values from 0.1 to 1.9
- attn_out: bfloat16 [512, 1024], P('tp', 'sp'), may hold values from -1.5 to 1.5
- delta_out: bfloat16 [512, 1024], P('tp', 'sp'), may hold values from -0.25 to 0.25
Outputs:
- mixed: bfloat16 [1024, 1024], P(('sp', 'tp'))
All inputs are finite; a program needn't handle non-finite values.
Results may differ from a plain program's by a relative error of at most 0.0045.
Values may be sent and summed in bfloat16 or wider, within the bound.
A program may use at most 64 MiB of HBM per device.

v0:
```python
import functools

import jax
import jax.numpy as jnp
from jax import lax
from jax.experimental import pallas as pl
from jax.experimental.pallas import tpu as pltpu
from jax.sharding import PartitionSpec as P

HEAD_DIM = 64
WINDOW = 64
norm_eps = 1e-06
MESH = pl.DeviceIdType.MESH
F32 = jnp.float32
BF16 = jnp.bfloat16
SUM_DTYPE = jnp.bfloat16
PARTS = 3


def exact(a, b, dims=((1,), (0,))):
    return lax.dot_general(
        a, b, (dims, ((), ())), precision=lax.Precision.HIGHEST, preferred_element_type=F32
    )


def plain(a, b, dims=((1,), (0,))):
    return lax.dot_general(a, b, (dims, ((), ())), preferred_element_type=F32)


def split(x):
    high = x.astype(BF16)
    return high, (x - high.astype(F32)).astype(BF16)


def close(a, b, dims=((1,), (0,))):
    (ca,), (cb,) = dims
    left = jnp.concatenate([a[0], a[1], a[0]], axis=ca)
    right = jnp.concatenate([b[0], b[0], b[1]], axis=cb)
    return plain(left, right, dims)


def near(a, b, dims=((1,), (0,))):
    a, b = split(a), split(b)
    return plain(a[0], b[0], dims) + (plain(a[1], b[0], dims) + plain(a[0], b[1], dims))


def silu(x):
    return x * jax.nn.sigmoid(x)


def unit_rows(x):
    return x * lax.rsqrt(jnp.sum(x * x, axis=-1, keepdims=True) + norm_eps)


def copy_to(src, dst, send, recv, device):
    return pltpu.make_async_remote_copy(
        src_ref=src,
        dst_ref=dst,
        send_sem=send,
        recv_sem=recv,
        device_id=device,
        device_id_type=MESH,
    )


class Gather:
    def __init__(self, n, me, tp, buf, send, recv, parts):
        self.nh = n // 2
        self.me, self.tp = me, tp
        self.lo, self.hi = lax.rem(me, 2), lax.div(me, 2)
        self.buf, self.send, self.recv = buf, send, recv
        self.parts = parts
        self.size = buf.shape[2] // parts

    def copy(self, b, route, p):
        target = (self.me + 2, self.me - 2, self.hi * 2 + 1 - self.lo)[route]
        cols = pl.ds(p * self.size, self.size)
        return copy_to(
            self.buf.at[b, :, cols],
            self.buf.at[b, :, cols],
            self.send.at[route, b, p],
            self.recv.at[b, p],
            (target, self.tp),
        )

    def can(self, route):
        return self.hi < self.nh - 1 if route == 0 else self.hi > 0

    def first(self, act):
        for p in range(self.parts):
            for route in (0, 1):
                pl.when(self.can(route))(lambda p=p, route=route: act(self.copy(self.me, route, p)))
            act(self.copy(self.me, 2, p))

    def begin(self):
        self.first(lambda c: c.start())

    def sides(self, d):
        return ((0, self.hi - d, self.hi - d >= 0), (1, self.hi + d, self.hi + d < self.nh))

    def step(self, d, use=None):
        for p in range(self.parts):
            if d < self.nh:
                for route, there, ok in self.sides(d):

                    @pl.when(ok)
                    def _(route=route, there=there):
                        b = there * 2 + self.lo
                        self.copy(b, 2, p).wait_recv()
                        pl.when(self.can(route))(lambda: self.copy(b, route, p).start())
                        self.copy(b, 2, p).start()
                        if use is not None:
                            use(b, p)

            for i, (_, there, ok) in enumerate(self.sides(d - 1)):
                if d == 1 and i == 1:
                    continue

                @pl.when(ok)
                def _(there=there):
                    b = there * 2 + 1 - self.lo
                    self.copy(b, 2, p).wait_recv()
                    if use is not None:
                        use(b, p)

    def drain(self):
        self.first(lambda c: c.wait_send())
        for d in range(1, self.nh):
            for p in range(self.parts):
                for route, there, ok in self.sides(d):

                    @pl.when(ok)
                    def _(route=route, there=there):
                        b = there * 2 + self.lo
                        pl.when(self.can(route))(lambda: self.copy(b, route, p).wait_send())
                        self.copy(b, 2, p).wait_send()


def layer_kernel(
    n, nt, heads, kvs, dheads,
    tok, gain_in, aq, ak, av, dq, dk, dv, dz, ao, do, ab, par, og_in, out,
    gain, og, kvw, in_sem, tokbuf, normed, wbuf, obuf, abbuf, acc, kvbuf, st, stbuf, o_loc, r_mat, joined, part, rsbuf,
    tok_s, tok_r, w_s, w_r, o_s, o_r, ab_s, ab_r, kv_s, kv_r, st_s, st_r, rs_s, rs_r,
):
    me, t = lax.axis_index("sp"), lax.axis_index("tp")
    rows, width = tok.shape
    kb = aq.shape[0]
    hd = HEAD_DIM
    aw, kw, dw = heads * hd, kvs * hd, dheads * hd
    mine = [(tok, tokbuf.at[t])]
    at = 0
    for w in (aq, dq, dk, dv, dz):
        mine.append((w, wbuf.at[me, :, pl.ds(at, w.shape[1])]))
        at += w.shape[1]
    mine += [(ak, kvw.at[pl.ds(0, kw)]), (av, kvw.at[pl.ds(kw, kw)]), (gain_in, gain), (og_in, og)]
    mine += [(ao, obuf.at[me, pl.ds(0, aw)]), (do, obuf.at[me, pl.ds(aw, dw)])]
    mine = [pltpu.make_async_copy(a, b, in_sem.at[i]) for i, (a, b) in enumerate(mine)]
    for c in mine:
        c.start()
    bar = pltpu.get_barrier_semaphore()
    for d in range(1, n):
        pl.semaphore_signal(bar, inc=1, device_id=(lax.rem(me + d, n), t), device_id_type=MESH)
    for d in range(1, nt):
        pl.semaphore_signal(bar, inc=1, device_id=(me, lax.rem(t + d, nt)), device_id_type=MESH)
    pl.semaphore_wait(bar, n - 1 + nt - 1)

    for c in mine:
        c.wait()
    wbuf[me, :, at:] = kvw[...].T
    tok_copies = [
        copy_to(tokbuf.at[t], tokbuf.at[t], tok_s.at[d - 1], tok_r.at[t], (me, lax.rem(t + d, nt)))
        for d in range(1, nt)
    ]
    for c in tok_copies:
        c.start()
    wg = Gather(n, me, t, wbuf, w_s, w_r, PARTS)
    ogather = Gather(n, me, t, obuf, o_s, o_r, 1)
    wg.begin()

    def ab_copy(d):
        p = lax.rem(me + d, n)
        return copy_to(ab, abbuf.at[me], ab_s.at[d], ab_r.at[me], (p, t))

    for d in range(1, n):
        ab_copy(d).start()
    abbuf[me] = ab[...]
    for d in range(1, nt):
        j = lax.rem(t + d, nt)
        copy_to(tokbuf.at[t], tokbuf.at[j], tok_s.at[d - 1], tok_r.at[j], (me, j)).wait_recv()
    total = jnp.zeros((rows, 1), F32)
    for j in range(nt):
        x = tokbuf[j].astype(F32)
        total += jnp.sum(x * x, axis=-1, keepdims=True)
    inverse = lax.rsqrt(total / (nt * width) + norm_eps)
    per = width // kb
    for j in range(nt):
        x = (tokbuf[j].astype(F32) * inverse * gain[:, j * width : (j + 1) * width]).astype(BF16)
        for i in range(per):
            normed[j * per + i] = x[:, i * kb : (i + 1) * kb]
    acc[...] = plain(normed[me], wbuf[me])

    half = wbuf.shape[2] // PARTS

    def use(b, p):
        cols = slice(p * half, (p + 1) * half)
        acc[:, cols] += plain(normed[b], wbuf[b, :, cols])

    for d in range(1, n // 2 + 1):
        wg.step(d, use)
    ogather.begin()

    kvbuf[WINDOW : WINDOW + rows] = acc[:, aw + 4 * dw :].astype(BF16)

    @pl.when(me == 0)
    def _():
        kvbuf[:WINDOW] = jnp.zeros((WINDOW, 2 * kw), BF16)

    @pl.when(me == n - 1)
    def _():
        kvbuf[WINDOW + rows :] = jnp.zeros((WINDOW, 2 * kw), BF16)

    base = aw
    for d in range(1, n):
        p = lax.rem(me + d, n)
        copy_to(ab, abbuf.at[p], ab_s.at[d], ab_r.at[p], (p, t)).wait_recv()
    tail = plain(abbuf[0], normed[0], ((1,), (1,)))
    for b in range(1, n):
        tail += plain(abbuf[b], normed[b], ((1,), (1,)))
    beta_t = jax.nn.sigmoid(tail + par[:, 0:1])
    soft = jnp.maximum(tail, 0.0) + jnp.log1p(jnp.exp(-jnp.abs(tail)))
    g_t = par[:, 1:2] * soft
    ri = lax.broadcasted_iota(jnp.int32, (rows, rows), 0)
    ci = lax.broadcasted_iota(jnp.int32, (rows, rows), 1)
    incl = (ri >= ci, ri <= ci)
    strict = (ri > ci, ri < ci)
    na = ab.shape[0]
    cum_t = [exact(g_t, jnp.where(m, 1.0, 0.0).astype(F32)) for m in (incl[1], incl[0])]
    stack = [beta_t] + cum_t
    if 3 * na < 128:
        stack.append(jnp.zeros((128 - 3 * na, rows), F32))
    columns = jnp.concatenate(stack, axis=0).T

    def head_to(p):
        up = copy_to(
            kvbuf.at[pl.ds(rows, WINDOW)], kvbuf.at[pl.ds(0, WINDOW)],
            kv_s.at[0], kv_r.at[0], (me + 1, t),
        )
        down = copy_to(
            kvbuf.at[pl.ds(WINDOW, WINDOW)], kvbuf.at[pl.ds(WINDOW + rows, WINDOW)],
            kv_s.at[1], kv_r.at[1], (me - 1, t),
        )
        return (up, down)[p]

    pl.when(me < n - 1)(lambda: head_to(0).start())
    pl.when(me > 0)(lambda: head_to(1).start())

    chains = []
    qs = []
    for h in range(dheads):
        def cols(i):
            lo_c = base + i * dw + h * hd
            return acc[:, lo_c : lo_c + hd].astype(BF16).astype(F32)

        q = unit_rows(silu(cols(0))) * hd ** (-0.5)
        k = unit_rows(silu(cols(1)))
        v = silu(cols(2))
        kk = near(k, k, ((1,), (1,)))
        qk = near(q, k, ((1,), (1,)))
        for r in range(2):
            c = h * 2 + r
            lane = 2 * dheads + c
            at = (1 + r) * na + lane
            gcol = columns[:, at : at + 1]
            grow = cum_t[r][lane : lane + 1, :]
            beta = columns[:, c : c + 1]
            decay = jnp.where(incl[r], jnp.exp(jnp.minimum(gcol - grow, 0.0)), 0.0)
            a = jnp.where(strict[r], beta * kk * decay, 0.0)
            eg = jnp.exp(gcol)
            last = gcol[rows - 1 : rows, :] if r == 0 else gcol[0:1, :]
            chains.append(
                dict(
                    r=r, h=h, a=a, rhs=jnp.concatenate([beta * v, beta * k * eg], axis=1),
                    pm=qk * decay, qe=q * eg, kd=(k * jnp.exp(last - gcol)).T, last=last,
                )
            )
    size = 1
    while (1 << size) <= rows:
        size += 1
    levels = size - 1
    eye = jnp.where(ri == ci, 1.0, 0.0).astype(F32)
    xor = ri ^ ci
    inv = [eye - jnp.where(xor == 1, ch["a"], 0.0) for ch in chains]
    pairs = [split(ch["a"]) for ch in chains]
    ogather.step(1)
    for lv in range(1, levels):
        m = jnp.where((xor >> lv) == 1, 1.0, 0.0).astype(BF16)
        xs = [split(x) for x in inv]
        left = [close(x, (m * a[0], m * a[1])) for x, a in zip(xs, pairs)]
        inv = [x - close(split(y), z) for x, y, z in zip(inv, left, xs)]
    sols = [split(close(split(x), split(ch["rhs"]))) for x, ch in zip(inv, chains)]
    outs = [close(split(ch["kd"]), s) for ch, s in zip(chains, sols)]
    e64 = jnp.where(
        lax.broadcasted_iota(jnp.int32, (hd, hd), 0)
        == lax.broadcasted_iota(jnp.int32, (hd, hd), 1), 1.0, 0.0,
    ).astype(F32)
    for ch, s in zip(chains, outs):
        full = jnp.concatenate([s[:, :hd], jnp.exp(ch["last"]) * e64 - s[:, hd:]], axis=1)
        st[ch["r"], ch["h"]] = full.astype(BF16)
    def state_copy(r, p):
        return copy_to(st.at[r], stbuf.at[me], st_s.at[p], st_r.at[me], (p, t))

    def state_all(act):
        for d in range(n - 1, 0, -1):
            pl.when(me + d < n)(lambda d=d: act(state_copy(0, me + d)))
            pl.when(me - d >= 0)(lambda d=d: act(state_copy(1, me - d)))

    state_all(lambda c: c.start())
    inner = [close(split(ch["pm"]), s) for ch, s in zip(chains, sols)]
    for ch, s in zip(chains, inner):
        o_loc[ch["r"], ch["h"]] = s[:, :hd]
        r_mat[ch["r"], ch["h"]] = ch["qe"] - s[:, hd:]


    ogather.step(2)

    pl.when(me > 0)(lambda: head_to(0).wait_recv())
    pl.when(me < n - 1)(lambda: head_to(1).wait_recv())
    span = rows + 2 * WINDOW
    qi = lax.broadcasted_iota(jnp.int32, (rows, span), 0)
    kj = lax.broadcasted_iota(jnp.int32, (rows, span), 1) - WINDOW
    pos = kj + me * rows
    allowed = (jnp.abs(qi - kj) <= WINDOW) & (pos >= 0) & (pos < n * rows)
    for h in range(heads):
        g = h // (heads // kvs)
        q = acc[:, h * hd : (h + 1) * hd].astype(BF16)
        s = plain(q, kvbuf[:, g * hd : (g + 1) * hd], ((1,), (1,))) * hd ** (-0.5)
        s = jnp.where(allowed, s, -jnp.inf)
        sink = par[h : h + 1, 2:3]
        m = jnp.maximum(jnp.max(s, axis=-1, keepdims=True), sink)
        e = jnp.exp(s - m)
        p = e / (jnp.sum(e, axis=-1, keepdims=True) + jnp.exp(sink - m))
        o = plain(p.astype(BF16), kvbuf[:, kw + g * hd : kw + (g + 1) * hd])
        joined[:, h * hd : (h + 1) * hd] = o.astype(BF16)
    for d in range(3, n // 2):
        ogather.step(d)

    for i in range(n):

        @pl.when(me != i)
        def _(i=i):
            copy_to(st.at[0], stbuf.at[i], st_s.at[i], st_r.at[i], (me, t)).wait_recv()

    fore = [jnp.zeros((hd, hd), F32)] * dheads
    back = [jnp.zeros((hd, hd), F32)] * dheads

    def enter(i, state, h, ok):
        both = jnp.where(ok, stbuf[i, h].astype(F32), ident)
        move, (high, low) = both[:, hd:].astype(BF16), split(state)
        return plain(move, high) + plain(move, low) + both[:, :hd]

    ident = jnp.concatenate([jnp.zeros((hd, hd), F32), e64], axis=1)
    for i in range(n - 1):
        fore = [enter(i, x, h, i < me) for h, x in enumerate(fore)]
        back = [enter(n - 1 - i, x, h, n - 1 - i > me) for h, x in enumerate(back)]
    if n // 2 > 2:
        ogather.step(n // 2)
    for h in range(dheads):
        o = o_loc[0, h] + o_loc[1, h] + near(r_mat[0, h], fore[h]) + near(r_mat[1, h], back[h])
        o = o * lax.rsqrt(jnp.mean(o * o, axis=-1, keepdims=True) + norm_eps) * og[...]
        lo_c = base + 3 * dw + h * hd
        gate = acc[:, lo_c : lo_c + hd].astype(BF16).astype(F32)
        joined[:, aw + h * hd : aw + (h + 1) * hd] = (o * silu(gate)).astype(BF16)

    cw = ao.shape[1]
    tr = rows // nt
    lhs = joined[...]
    for b in range(n):
        y = plain(lhs, obuf[b])
        for j in range(nt):
            part[j, :, b * cw : (b + 1) * cw] = y[j * tr : (j + 1) * tr].astype(SUM_DTYPE)
    rs_copies = [
        copy_to(
            part.at[lax.rem(t + d, nt)], rsbuf.at[d - 1], rs_s.at[d - 1], rs_r.at[d - 1],
            (me, lax.rem(t + d, nt)),
        )
        for d in range(1, nt)
    ]
    for c in rs_copies:
        c.start()
    own = joined[pl.ds(pl.multiple_of(t * tr, tr), tr)]
    for c in tok_copies:
        c.wait_send()
    for d in range(1, n):
        ab_copy(d).wait_send()
    wg.drain()
    ogather.drain()
    pl.when(me < n - 1)(lambda: head_to(0).wait_send())
    pl.when(me > 0)(lambda: head_to(1).wait_send())
    state_all(lambda c: c.wait_send())
    total = jnp.concatenate([plain(own, obuf[b]) for b in range(n)], axis=1)
    for d in range(1, nt):
        rs_copies[d - 1].wait_recv()
        total += rsbuf[d - 1].astype(F32)
    out[...] = total.astype(BF16)
    for c in rs_copies:
        c.wait_send()


def per_device(
    tokens, norm_gain, attn_query, attn_key, attn_value, sink_logit, delta_query, delta_key,
    delta_value, delta_gate, beta_weight, decay_weight, beta_shift, decay_log, out_gain,
    attn_out, delta_out,
):
    n, nt = lax.axis_size("sp"), lax.axis_size("tp")
    rows, width = tokens.shape
    kb = attn_query.shape[0]
    heads, kvs = attn_query.shape[1] // HEAD_DIM, attn_key.shape[1] // HEAD_DIM
    dheads = delta_query.shape[1] // HEAD_DIM
    ab = 2 * dheads
    wide = (2 * kvs + heads + 4 * dheads) * HEAD_DIM
    na = -(-2 * ab // 16) * 16
    gates = jnp.concatenate(
        [
            beta_weight.reshape(kb, ab).T, decay_weight.reshape(kb, ab).T,
            jnp.zeros((na - 2 * ab, kb), BF16),
        ],
        axis=0,
    )
    flat = lambda a, before: jnp.pad(a, (before, na - before - a.shape[0]))
    par = jnp.stack(
        [
            flat(beta_shift.T.reshape(ab), 0),
            flat(-jnp.exp(decay_log.T.reshape(ab)) / (rows * n), ab),
            flat(sink_logit, 0),
        ],
        axis=1,
    )
    cw = attn_out.shape[1]
    tr = rows // nt
    hd = HEAD_DIM
    kw = kvs * hd
    dma = pltpu.SemaphoreType.DMA
    vm = pl.BlockSpec(memory_space=pltpu.VMEM)
    hbm = pl.BlockSpec(memory_space=pltpu.HBM)
    return pl.pallas_call(
        functools.partial(layer_kernel, n, nt, heads, kvs, dheads),
        out_shape=jax.ShapeDtypeStruct((tr, n * cw), BF16),
        in_specs=[hbm] * 11 + [vm] * 2 + [hbm],
        out_specs=vm,
        scratch_shapes=[
            pltpu.VMEM((1, nt * width), F32),
            pltpu.VMEM((1, hd), F32),
            pltpu.VMEM((2 * kw, kb), BF16),
            dma((12,)),
            pltpu.VMEM((nt, rows, width), BF16),
            pltpu.VMEM((n, rows, kb), BF16),
            pltpu.VMEM((n, kb, wide), BF16),
            pltpu.VMEM((n, (heads + dheads) * hd, cw), BF16),
            pltpu.VMEM((n, na, kb), BF16),
            pltpu.VMEM((rows, wide), F32),
            pltpu.VMEM((rows + 2 * WINDOW, 2 * kw), BF16),
            pltpu.VMEM((2, dheads, hd, 2 * hd), BF16),
            pltpu.VMEM((n, dheads, hd, 2 * hd), BF16),
            pltpu.VMEM((2, dheads, rows, hd), F32),
            pltpu.VMEM((2, dheads, rows, hd), F32),
            pltpu.VMEM((rows, (heads + dheads) * hd), BF16),
            pltpu.VMEM((nt, tr, n * cw), SUM_DTYPE),
            pltpu.VMEM((nt - 1, tr, n * cw), SUM_DTYPE),
            dma((nt - 1,)), dma((nt,)),
            dma((3, n, PARTS)), dma((n, PARTS)),
            dma((3, n, 1)), dma((n, 1)),
            dma((n,)), dma((n,)),
            dma((2,)), dma((2,)),
            dma((n,)), dma((n,)),
            dma((nt - 1,)), dma((nt - 1,)),
        ],
        compiler_params=pltpu.CompilerParams(
            collective_id=0, has_side_effects=True, vmem_limit_bytes=60 * 1024 * 1024
        ),
    )(
        tokens, norm_gain.reshape(1, nt * width), attn_query, attn_key.T, attn_value.T, delta_query,
        delta_key, delta_value, delta_gate, attn_out, delta_out, gates, par,
        out_gain.reshape(1, hd),
    )


def solution(mesh):
    return jax.shard_map(
        per_device,
        mesh=mesh,
        in_specs=(
            P("sp", "tp"), P(), P("sp", "tp"), P("sp", "tp"), P("sp", "tp"), P("tp"),
            P("sp", "tp"), P("sp", "tp"), P("sp", "tp"), P("sp", "tp"),
            P("sp", "tp", None), P("sp", "tp", None), P(None, "tp"), P(None, "tp"), P(),
            P("tp", "sp"), P("tp", "sp"),
        ),
        out_specs=P(("sp", "tp"), None),
        check_vma=False,
    )
```

profile of v0, /device:TPU:0, one launch (start us, length us, event | category | flops | bytes accessed | tf_op | source)
XLA Modules:
  0.0 54.6 jit_solution(16280996725626732762)
XLA Ops:
  0.0 0.0 copy-start
  0.0 0.1 pad.20.clone
  0.1 0.6 %copy-done = f32[2,2]{1,0:T(2,128)S(1)} copy-done((f32[2,2]{1,0:T(2,128)S(1)}, f32[2,2]{1,0:T(2,128)}, u32[]{:S(2)}) %copy-start) | copy-done | bytes 40
  0.7 0.1 copy.23
  0.8 0.1 reshape.23
  0.9 0.0 copy-start.1
  0.9 0.7 %copy-done.1 = f32[2,2]{1,0:T(2,128)S(1)} copy-done((f32[2,2]{1,0:T(2,128)S(1)}, f32[2,2]{1,0:T(2,128)}, u32[]{:S(2)}) %copy-start.1) | copy-done | bytes 40
  1.5 0.1 copy.24
  1.6 0.0 copy-start.4
  1.6 0.1 div.9
  1.7 0.6 %copy-done.4 = f32[2]{0:T(128)S(1)} copy-done((f32[2]{0:T(128)S(1)}, f32[2]{0:T(128)}, u32[]{:S(2)}) %copy-start.4) | copy-done | bytes 32
  2.3 0.1 pad_bitcast_fusion
  2.4 0.0 copy-start.2
  2.4 0.0 copy-start.3
  2.4 0.7 %copy-done.2 = bf16[128,2,2]{0,2,1:T(2,128)(2,1)S(1)} copy-done((bf16[128,2,2]{0,2,1:T(2,128)(2,1)S(1)}, bf16[128,2,2]{0,2,1:T(2,128)(2,1)}, u32[]{:S(2)}) %copy-start.2) | copy-done | bytes 1048
  3.1 0.0 copy-done.3
  3.1 0.7 %maximum_maximum_fusion.ab = bf16[16,128]{1,0:T(8,128)(2,1)} fusion(bf16[4,128]{1,0:T(4,128)(2,1)S(1)} %bitcast.23, bf16[4,128]{1,0:T(4,128)(2,1)S(1)} %bitcast.24, bf16[16]{0:T(256)(128)(2,1)S(1)} %pad.20.clone), kind=kLoop, calls=%fused_computation | loop fusion | flops 12288 | bytes 6176 | tf_op jit(solution)/shard_map/concatenate | solution.py:422
  3.7 0.7 %copy.25.par = f32[16,3]{1,0:T(8,128)} copy(f32[16,3]{0,1:T(4,128)S(1)} %pad_maximum_fusion) | data formatting | bytes 384 | tf_op jit(solution)/shard_map/stack | solution.py:430
  4.4 48.7 %shard_map.163 = bf16[32,1024]{1,0:T(8,128)(2,1)} custom-call(bf16[128,256]{1,0:T(8,128)(2,1)} %tok.1, f32[1,1024]{1,0:T(1,128)} %bitcast.21, bf16[128,128]{1,0:T(8,128)(2,1)} %aq.1, bf16[64,128]{1,0:T(8,128)(2,1)} %bitcast.19, bf16[64,128]{1,0:T(8,128)(2,1)} %bitcast.20, bf16[128,128]{1,0:T(8,128)(2,1)} %dq.1, bf16[128,128]{1,0:T(8,128)(2,1)} %dk.1, ...), custom_call_target="tpu_custom_call" | custom-call | tf_op jit(solution)/shard_map/pallas_call | solution.py:445
  53.1 1.5 %copy.27 = bf16[32,1024]{1,0:T(8,128)(2,1)} copy(bf16[32,1024]{1,0:T(8,128)(2,1)} %shard_map.163) | data formatting | bytes 131072
  (4 shorter events, 0.0 us)
Async XLA Ops:
  0.0 0.7 %copy-start = (f32[2,2]{1,0:T(2,128)S(1)}, f32[2,2]{1,0:T(2,128)}, u32[]{:S(2)}) copy-start(f32[2,2]{1,0:T(2,128)} %param.29) | copy-start | bytes 52
  0.9 0.7 %copy-start.1 = (f32[2,2]{1,0:T(2,128)S(1)}, f32[2,2]{1,0:T(2,128)}, u32[]{:S(2)}) copy-start(f32[2,2]{1,0:T(2,128)} %param.30) | copy-start | bytes 52
  1.6 0.7 %copy-start.4 = (f32[2]{0:T(128)S(1)}, f32[2]{0:T(128)}, u32[]{:S(2)}) copy-start(f32[2]{0:T(128)} %param.22) | copy-start | bytes 28
  2.4 0.7 %copy-start.2 = (bf16[128,2,2]{0,2,1:T(2,128)(2,1)S(1)}, bf16[128,2,2]{0,2,1:T(2,128)(2,1)}, u32[]{:S(2)}) copy-start(bf16[128,2,2]{0,2,1:T(2,128)(2,1)} %param.28) | copy-start | bytes 3076
  2.4 0.7 %copy-start.3 = (bf16[128,2,2]{0,2,1:T(2,128)(2,1)S(1)}, bf16[128,2,2]{0,2,1:T(2,128)(2,1)}, u32[]{:S(2)}) copy-start(bf16[128,2,2]{0,2,1:T(2,128)(2,1)} %param.27) | copy-start | bytes 3076
where the time goes:
time: 54.9 us; the launch traced here: 54.6 us
  Pallas kernels  48.7 us (89%)
  local copies, waits for them, and re-layouts  5.2 us (9%)
  other arithmetic  0.67 us (1%)
    pallas_call x1, Pallas kernels, per_device(): pl.pallas_call(functools.partial(layer_kernel, n, nt, heads, kvs, dheads)...  48.7 us
    unnamed x11, local copies, waits for them, and re-layouts  4.01 us

commit v1 on v0

--- a/solution.py
+++ b/solution.py
@@ -387,7 +387,6 @@
     ]
     for c in rs_copies:
         c.start()
-    own = joined[pl.ds(pl.multiple_of(t * tr, tr), tr)]
     for c in tok_copies:
         c.wait_send()
     for d in range(1, n):
@@ -397,7 +396,7 @@
     pl.when(me < n - 1)(lambda: head_to(0).wait_send())
     pl.when(me > 0)(lambda: head_to(1).wait_send())
     state_all(lambda c: c.wait_send())
-    total = jnp.concatenate([plain(own, obuf[b]) for b in range(n)], axis=1)
+    total = part[t].astype(F32)
     for d in range(1, nt):
         rs_copies[d - 1].wait_recv()
         total += rsbuf[d - 1].astype(F32)

time: 54.9 us -> 54.9 us (level)
  no operation moved by 1% of the time
where the time goes in v1:
time: 54.9 us; the launch traced here: 54.6 us
  Pallas kernels  48.7 us (89%)
  local copies, waits for them, and re-layouts  5.2 us (9%)
  other arithmetic  0.67 us (1%)
    pallas_call x1, Pallas kernels, per_device(): pl.pallas_call(functools.partial(layer_kernel, n, nt, heads, kvs, dheads)...  48.7 us
    unnamed x11, local copies, waits for them, and re-layouts  4.01 us

profile of v1, /device:TPU:0, one launch (start us, length us, event | category | flops | bytes accessed | tf_op | source)
XLA Modules:
  0.0 54.6 jit_solution(8971000449733264330)
XLA Ops:
  0.0 0.0 copy-start
  0.0 0.1 pad.20.clone
  0.1 0.6 %copy-done = f32[2,2]{1,0:T(2,128)S(1)} copy-done((f32[2,2]{1,0:T(2,128)S(1)}, f32[2,2]{1,0:T(2,128)}, u32[]{:S(2)}) %copy-start) | copy-done | bytes 40
  0.7 0.1 copy.23
  0.8 0.1 reshape.23
  0.9 0.0 copy-start.1
  0.9 0.7 %copy-done.1 = f32[2,2]{1,0:T(2,128)S(1)} copy-done((f32[2,2]{1,0:T(2,128)S(1)}, f32[2,2]{1,0:T(2,128)}, u32[]{:S(2)}) %copy-start.1) | copy-done | bytes 40
  1.5 0.1 copy.24
  1.6 0.0 copy-start.4
  1.6 0.1 div.9
  1.7 0.6 %copy-done.4 = f32[2]{0:T(128)S(1)} copy-done((f32[2]{0:T(128)S(1)}, f32[2]{0:T(128)}, u32[]{:S(2)}) %copy-start.4) | copy-done | bytes 32
  2.3 0.1 pad_bitcast_fusion
  2.4 0.0 copy-start.2
  2.4 0.0 copy-start.3
  2.4 0.7 %copy-done.2 = bf16[128,2,2]{0,2,1:T(2,128)(2,1)S(1)} copy-done((bf16[128,2,2]{0,2,1:T(2,128)(2,1)S(1)}, bf16[128,2,2]{0,2,1:T(2,128)(2,1)}, u32[]{:S(2)}) %copy-start.2) | copy-done | bytes 1048
  3.1 0.0 copy-done.3
  3.1 0.7 %maximum_maximum_fusion.ab = bf16[16,128]{1,0:T(8,128)(2,1)} fusion(bf16[4,128]{1,0:T(4,128)(2,1)S(1)} %bitcast.23, bf16[4,128]{1,0:T(4,128)(2,1)S(1)} %bitcast.24, bf16[16]{0:T(256)(128)(2,1)S(1)} %pad.20.clone), kind=kLoop, calls=%fused_computation | loop fusion | flops 12288 | bytes 6176 | tf_op jit(solution)/shard_map/concatenate | solution.py:421
  3.7 0.7 %copy.25.par = f32[16,3]{1,0:T(8,128)} copy(f32[16,3]{0,1:T(4,128)S(1)} %pad_maximum_fusion) | data formatting | bytes 384 | tf_op jit(solution)/shard_map/stack | solution.py:429
  4.4 48.7 %shard_map.163 = bf16[32,1024]{1,0:T(8,128)(2,1)} custom-call(bf16[128,256]{1,0:T(8,128)(2,1)} %tok.1, f32[1,1024]{1,0:T(1,128)} %bitcast.21, bf16[128,128]{1,0:T(8,128)(2,1)} %aq.1, bf16[64,128]{1,0:T(8,128)(2,1)} %bitcast.19, bf16[64,128]{1,0:T(8,128)(2,1)} %bitcast.20, bf16[128,128]{1,0:T(8,128)(2,1)} %dq.1, bf16[128,128]{1,0:T(8,128)(2,1)} %dk.1, ...), custom_call_target="tpu_custom_call" | custom-call | tf_op jit(solution)/shard_map/pallas_call | solution.py:444
  53.1 1.5 %copy.27 = bf16[32,1024]{1,0:T(8,128)(2,1)} copy(bf16[32,1024]{1,0:T(8,128)(2,1)} %shard_map.163) | data formatting | bytes 131072
  (4 shorter events, 0.0 us)
Async XLA Ops:
  0.0 0.7 %copy-start = (f32[2,2]{1,0:T(2,128)S(1)}, f32[2,2]{1,0:T(2,128)}, u32[]{:S(2)}) copy-start(f32[2,2]{1,0:T(2,128)} %param.29) | copy-start | bytes 52
  0.9 0.7 %copy-start.1 = (f32[2,2]{1,0:T(2,128)S(1)}, f32[2,2]{1,0:T(2,128)}, u32[]{:S(2)}) copy-start(f32[2,2]{1,0:T(2,128)} %param.30) | copy-start | bytes 52
  1.6 0.7 %copy-start.4 = (f32[2]{0:T(128)S(1)}, f32[2]{0:T(128)}, u32[]{:S(2)}) copy-start(f32[2]{0:T(128)} %param.22) | copy-start | bytes 28
  2.4 0.7 %copy-start.2 = (bf16[128,2,2]{0,2,1:T(2,128)(2,1)S(1)}, bf16[128,2,2]{0,2,1:T(2,128)(2,1)}, u32[]{:S(2)}) copy-start(bf16[128,2,2]{0,2,1:T(2,128)(2,1)} %param.28) | copy-start | bytes 3076
  2.4 0.7 %copy-start.3 = (bf16[128,2,2]{0,2,1:T(2,128)(2,1)S(1)}, bf16[128,2,2]{0,2,1:T(2,128)(2,1)}, u32[]{:S(2)}) copy-start(bf16[128,2,2]{0,2,1:T(2,128)(2,1)} %param.27) | copy-start | bytes 3076
